TPU v7x, 32 devices: a whole 2x2x4 slice. The times are simulated.
32 devices in a mesh: ep: 8 (over z, y), tp: 4 (over x, core).
Axes of the slice: x: 2, y: 2, z: 4, core: 2. Of those that a mesh axis runs over, the one named last changes fastest.
Arguments:
- query_rows: bfloat16 [16384, 1024], P('ep', 'tp'), may hold values from -6 to 6
- key_rows: bfloat16 [16384, 1024], P('ep', 'tp'), may hold values from -6 to 6
- value_rows: bfloat16 [16384, 2048], P('ep', 'tp'), may hold values from -6 to 6
- gate_rows: bfloat16 [16384, 2048], P('ep', 'tp'), may hold values from -6 to 6
- log_decay: float32 [8, 16384], P('tp', 'ep'), may hold values from -1 to 0
- out_proj: bfloat16 [2048, 2048], P('tp'), may hold values from -0.125 to 0.125
- moe_input: bfloat16 [4096, 2048], P(('ep', 'tp')), may hold values from -6 to 6
- norm_gain: float32 [2048], replicated, may hold values from 0.1 to 1.9
- routing: int32 [4096, 4], P(('ep', 'tp')), may hold values from 0 to 31, all different within a row; in each aligned block of 128 rows (0 to 127, 128 to 255, ...) at most 32 rows name the same one
- route_weight: float32 [4096, 4], P(('ep', 'tp')), may hold values from 0.2 to 1
- expert_gate: bfloat16 [32, 2048, 512], P(('ep', 'tp')), may hold values from -0.125 to 0.125
- expert_up: bfloat16 [32, 2048, 512], P(('ep', 'tp')), may hold values from -0.125 to 0.125
- expert_down: bfloat16 [32, 512, 2048], P(('ep', 'tp')), may hold values from -0.25 to 0.25
- shared_gate: bfloat16 [2048, 512], replicated, may hold values from -0.125 to 0.125
- shared_up: bfloat16 [2048, 512], replicated, may hold values from -0.125 to 0.125
- shared_down: bfloat16 [512, 2048], replicated, may hold values from -0.25 to 0.25
Outputs:
- mixer_out: bfloat16 [16384, 2048], P(('ep', 'tp'))
- moe_out: bfloat16 [4096, 2048], P(('ep', 'tp'))
Inputs may be any that keep to these rules, and one draw needn't show every extreme that they name: `routing`: within the rows of one device no expert is named more than 32 times.
All inputs are finite; a program needn't handle non-finite values.
Results may differ from a plain program's by a relative error of at most 0.019.
Values may be sent and summed in bfloat16 or wider, within the bound.
A program may use at most 128 MiB of HBM per device.

v0:
```python
import functools
import math

import jax
import jax.numpy as jnp
from jax import lax
from jax.experimental import pallas as pl
from jax.experimental.pallas import tpu as pltpu
from jax.sharding import PartitionSpec as P

DK = 128
DV = 256
BLOCK = 128
EPS = 1e-06
Z_GROUPS = 4

F32 = jnp.float32
BF16 = jnp.bfloat16
MESH = pl.DeviceIdType.MESH


def dot(a, b):
    return jnp.dot(a, b, preferred_element_type=F32)


def silu(v):
    return v / (1.0 + jnp.exp(-v))


def kernel(
    E, T, G, C,
    x_ref, gain_ref, meta_ref, cum_ref, cumc_ref, tot_ref,
    q_hbm, k_hbm, v_hbm, g_hbm, op_hbm,
    wg_hbm, wu_hbm, wd_hbm, sg_hbm, su_hbm, sd_hbm,
    mix_ref, moe_ref,
    q_v, k_v, v_v, g_v, op_v, wg_v, wu_v, wd_v,
    xz, mz, dsp, rcv, ret, dwt, shr, prcv,
    upd, sblk, lend, srcv, trcv, rs, rr, inc,
    load_sem,
    z_s, z_r, m_s, m_r, d_s, d_r, b_s, b_r, p_s, p_r, s_s, s_r, t_s, t_r,
    o1_s, o1_r, o2_s, o2_r, o3_s, o3_r, r_s, r_r,
):
    ep = lax.axis_index("ep")
    tp = lax.axis_index("tp")
    R = E // G
    Pn = R * T
    zi = ep // R
    yi = ep % R
    j = yi * T + tp
    tok, width = x_ref.shape
    n_visits = meta_ref.shape[0] // 2
    nb = cum_ref.shape[0]
    H = cum_ref.shape[1]
    nbc = nb // T
    B = math.gcd(T, 2)
    A = T // B
    ta, tb = tp // B, tp % B
    piece = op_v.shape[1] // R
    scale = DK ** (-0.5)

    loads = [
        pltpu.make_async_copy(src, dst, load_sem.at[i])
        for i, (src, dst) in enumerate(
            ((k_hbm, k_v), (v_hbm, v_v), (op_hbm, op_v.at[tp]), (sg_hbm, wg_v), (su_hbm, wu_v),
             (sd_hbm, wd_v), (q_hbm, q_v), (g_hbm, g_v), (wg_hbm.at[0], wg_v),
             (wu_hbm.at[0], wu_v), (wd_hbm.at[0], wd_v))
        )
    ]
    for c in loads[:8]:
        c.start()

    def z_place(g):
        return (g * R + yi, tp)

    def plane_peer(d):
        p = (j + d) % Pn
        return (zi * R + p // T, p % T)

    def tp_peer(i):
        return (ep, (tp + i) % T)

    barrier = pltpu.get_barrier_semaphore()

    @pl.loop(1, Pn)
    def _(d):
        pl.semaphore_signal(barrier, inc=1, device_id=plane_peer(d), device_id_type=MESH)

    @pl.loop(1, E)
    def _(d):
        pl.semaphore_signal(barrier, inc=1, device_id=((ep + d) % E, tp), device_id_type=MESH)

    xf = x_ref[...].astype(F32)
    xz[zi] = (
        xf * lax.rsqrt(jnp.mean(xf * xf, axis=-1, keepdims=True) + EPS) * gain_ref[...]
    ).astype(BF16)
    mz[zi] = meta_ref[...]
    pl.semaphore_wait(barrier, Pn - 1 + E - 1)

    def rcopy(src, dst, ss, rs_, dev):
        return pltpu.make_async_remote_copy(
            src_ref=src, dst_ref=dst, send_sem=ss, recv_sem=rs_, device_id=dev, device_id_type=MESH
        )

    def z_copy(g, way):
        to = (zi - 1, zi + 1)[way]
        return rcopy(xz.at[g], xz.at[g], z_s.at[way, g], z_r.at[g], z_place(to))

    def m_copy(g, way):
        to = (zi - 1, zi + 1)[way]
        return rcopy(mz.at[g], mz.at[g], m_s.at[way, g], m_r.at[g], z_place(to))

    def z_sends(g, way):
        if way:
            return (g <= zi) & (zi + 1 < G)
        return (g >= zi) & (zi > 0)

    def group_at(i):
        dist = (i + 1) // 2
        g = zi + jnp.where(i % 2 == 1, -dist, dist)
        return g, (g >= 0) & (g < G)

    def rows(d):
        return pl.ds(pl.multiple_of(d * C, C), C)

    def d_copy(r, d):
        return rcopy(dsp.at[r, rows(d)], rcv.at[r, rows(d)], d_s.at[r, d], d_r.at[r, d],
                     plane_peer(d))

    def b_copy(r, d):
        return rcopy(rcv.at[r, rows(d)], ret.at[r, rows(d)], b_s.at[r, d], b_r.at[r, d],
                     plane_peer(Pn - d))

    def p_copy(g):
        return rcopy(dsp.at[g, 0:tok], prcv.at[zi], p_s.at[g], p_r.at[zi], z_place(g))

    def p_arrival(g):
        return rcopy(dsp.at[g, 0:tok], prcv.at[g], p_s.at[g], p_r.at[g], z_place(g))

    def s_copy(d):
        return rcopy(lend, srcv.at[d - 1], s_s.at[d], s_r.at[d], ((ep + d) % E, tp))

    def t_copy(d):
        return rcopy(tot_ref, trcv.at[d], t_s.at[d], t_r.at[d], ((ep + d) % E, tp))

    def shard(da, db=0):
        return ((ta + A - da) % A) * B + (tb + B - db) % B

    def part(y):
        return pl.ds(pl.multiple_of(y * piece, piece), piece)

    def o1_copy(da, src):
        at = op_v.at[src, part(yi)]
        return rcopy(at, at, o1_s.at[da], o1_r.at[da], (ep, ((ta + da) % A) * B + tb))

    def o2_copy(da, dy, y):
        at = op_v.at[shard(da), part(y)]
        return rcopy(at, at, o2_s.at[da, dy], o2_r.at[da, dy], (zi * R + (yi + dy) % R, tp))

    def o3_copy(da, db, src):
        at = op_v.at[src]
        return rcopy(at, at, o3_s.at[da, db], o3_r.at[da, db], (ep, ta * B + (tb + db) % B))

    def r_copy(i):
        return rcopy(rs.at[i], rr.at[i - 1], r_s.at[i], r_r.at[i], tp_peer(i))

    for way in (0, 1):
        @pl.when(z_sends(zi, way))
        def _():
            m_copy(zi, way).start()
            z_copy(zi, way).start()

    def dispatch(r):
        meta = mz[r]
        owner = lax.broadcasted_iota(jnp.int32, (Pn, tok), 0)
        owner = (zi * Pn + (owner + j) % Pn).astype(F32)
        member = jnp.zeros((Pn, tok), F32)
        weight = jnp.zeros((Pn, tok), F32)
        for v in range(n_visits):
            hit = meta[v:v + 1, :] == owner
            member += jnp.where(hit, 1.0, 0.0)
            weight += jnp.where(hit, meta[n_visits + v:n_visits + v + 1, :], 0.0)
        before = lax.broadcasted_iota(jnp.int32, (tok, tok), 0) < lax.broadcasted_iota(
            jnp.int32, (tok, tok), 1
        )
        rank = dot(member.astype(BF16), jnp.where(before, 1.0, 0.0).astype(BF16))
        rank = jnp.where(member > 0.5, rank, -1.0)
        slot = lax.broadcasted_iota(jnp.int32, (C, tok), 0).astype(F32)
        picks, wts = [], []
        for d in range(Pn):
            eq = slot == rank[d:d + 1, :]
            picks.append(jnp.where(eq, 1.0, 0.0))
            wts.append(jnp.where(eq, weight[d:d + 1, :], 0.0))
        pick = jnp.concatenate(picks, axis=0).astype(BF16)
        dwt[r] = jnp.concatenate(wts, axis=0).T.astype(BF16)
        out = dot(pick, xz[r]).astype(BF16)
        dsp[r] = out
        rcv[r, 0:C] = out[0:C]

        @pl.loop(1, Pn)
        def _(d):
            d_copy(r, d).start()

    dispatch(zi)

    loads[0].wait()
    loads[1].wait()

    inc[...] = jnp.zeros_like(inc)

    @pl.loop(0, nb)
    def _(b):
        rb = pl.ds(pl.multiple_of(b * BLOCK, BLOCK), BLOCK)
        cumc = cumc_ref[b]
        crow = cum_ref[b]
        for h in range(H):
            col = cumc[:, h:h + 1]
            last = crow[h:h + 1, BLOCK - 1:BLOCK]
            u = (k_v[rb, h * DK:(h + 1) * DK].astype(F32) * (scale * jnp.exp(last - col))).astype(BF16)
            add = lax.dot_general(
                u, v_v[rb, h * DV:(h + 1) * DV], (((0,), (0,)), ((), ())),
                preferred_element_type=F32,
            )
            upd[b, h] = add
            inc[h] = inc[h] * jnp.exp(last) + add

    lend[...] = inc[...].astype(BF16)

    loads[3].wait()
    loads[4].wait()
    loads[5].wait()
    hid = (silu(dot(xz[zi], wg_v[...])) * dot(xz[zi], wu_v[...])).astype(BF16)
    shr[...] = dot(hid, wd_v[...])
    for c in loads[8:]:
        c.start()

    def serve(r):
        @pl.loop(1, Pn)
        def _(d):
            d_copy(r, d).wait_recv()

        rows_in = rcv[r]
        hidden = (silu(dot(rows_in, wg_v[...])) * dot(rows_in, wu_v[...])).astype(BF16)
        res = dot(hidden, wd_v[...]).astype(BF16)
        rcv[r] = res
        ret[r, 0:C] = res[0:C]

        @pl.loop(1, Pn)
        def _(d):
            b_copy(r, d).start()

    loads[8].wait()
    loads[9].wait()
    loads[10].wait()
    @pl.loop(1, 2 * G - 1)
    def _(i):
        g, there = group_at(i)

        @pl.when(there)
        def _():
            m_copy(g, 0).wait_recv()
            z_copy(g, 0).wait_recv()
            for way in (0, 1):
                @pl.when(z_sends(g, way))
                def _():
                    m_copy(g, way).start()
                    z_copy(g, way).start()
            dispatch(g)

        @pl.when(i == G - 1)
        def _():
            @pl.loop(1, E)
            def _(d):
                @pl.when(ep + d < E)
                def _():
                    t_copy(d).start()
                    s_copy(d).start()

        behind, known = group_at(i - 2)

        @pl.when(known & (i >= 2))
        def _():
            serve(behind)

    loads[2].wait()
    for da in range(1, A):
        o1_copy(da, tp).start()
    for i in (2 * G - 3, 2 * G - 2):
        g, there = group_at(jnp.int32(i))

        @pl.when(there)
        def _():
            serve(g)

    inc[...] = jnp.zeros_like(inc)

    @pl.loop(1, E)
    def _(i):
        d = E - i

        @pl.when(ep >= d)
        def _():
            t_copy(d).wait_recv()
            s_copy(d).wait_recv()
            for h in range(H):
                shrink = jnp.exp(trcv[d, h:h + 1, 0:1])
                inc[h] = inc[h] * shrink + srcv[d - 1, h].astype(F32)

    @pl.loop(0, nb)
    def _(b):
        crow = cum_ref[b]
        for h in range(H):
            s = inc[h]
            sblk[b, h] = s.astype(BF16)
            inc[h] = s * jnp.exp(crow[h:h + 1, BLOCK - 1:BLOCK]) + upd[b, h]

    loads[6].wait()
    loads[7].wait()
    causal = lax.broadcasted_iota(jnp.int32, (BLOCK, BLOCK), 0) >= lax.broadcasted_iota(
        jnp.int32, (BLOCK, BLOCK), 1
    )

    def retain(i):
        chunk = (tp + i) % T

        @pl.loop(0, nbc)
        def _(w):
            b = chunk * nbc + w
            rb = pl.ds(pl.multiple_of(b * BLOCK, BLOCK), BLOCK)
            ro = pl.ds(pl.multiple_of(w * BLOCK, BLOCK), BLOCK)
            cumc = cumc_ref[b]
            crow = cum_ref[b]
            for h in range(H):
                col = cumc[:, h:h + 1]
                row = crow[h:h + 1, :]
                qb = q_v[rb, h * DK:(h + 1) * DK]
                kb = k_v[rb, h * DK:(h + 1) * DK]
                vb = v_v[rb, h * DV:(h + 1) * DV]
                sc = lax.dot_general(qb, kb, (((1,), (1,)), ((), ())), preferred_element_type=F32)
                dec = jnp.exp(jnp.where(causal, col - row, 0.0))
                wt = jnp.where(causal, sc * scale * dec, 0.0).astype(BF16)
                raw = dot(wt, vb) + dot(qb, sblk[b, h]) * jnp.exp(col)
                avg = jnp.mean(raw, axis=-1, keepdims=True)
                cen = raw - avg
                var = jnp.mean(cen * cen, axis=-1, keepdims=True)
                gate = g_v[rb, h * DV:(h + 1) * DV].astype(F32)
                rs[i, ro, h * DV:(h + 1) * DV] = (
                    silu(gate) * (cen * lax.rsqrt(var + EPS))
                ).astype(BF16)

    @pl.loop(1, T)
    def _(i):
        retain(i)

    retain(0)

    @pl.loop(1, T)
    def _(i):
        r_copy(i).start()

    def combine(r):
        @pl.loop(1, Pn)
        def _(d):
            b_copy(r, d).wait_recv()

        @pl.loop(1, Pn)
        def _(d):
            d_copy(r, d).wait_send()

        dsp[r, 0:tok] = dot(dwt[r], ret[r]).astype(BF16)
        p_copy(r).start()

    @pl.loop(1, 2 * G - 1)
    def _(i):
        g, there = group_at(i)

        @pl.when(there)
        def _():
            combine(g)

    for da in range(1, A):
        o1_copy(da, shard(da)).wait_recv()
        for dy in range(1, R):
            o2_copy(da, dy, yi).start()
    for db in range(1, B):
        o3_copy(0, db, tp).start()

    for da in range(1, A):
        for dy in range(1, R):
            o2_copy(da, dy, (yi + R - dy) % R).wait_recv()
        for db in range(1, B):
            o3_copy(da, db, shard(da)).start()

    for da in range(A):
        for db in range(1, B):
            o3_copy(da, db, shard(da, db)).wait_recv()

    @pl.loop(1, T)
    def _(i):
        r_copy(i).wait_recv()

    n_col = 512
    @pl.loop(0, width // n_col)
    def _(n):
        cols = pl.ds(pl.multiple_of(n * n_col, n_col), n_col)
        acc = dot(rs[0], op_v[tp, :, cols])
        for i in range(1, T):
            acc += dot(rr[i - 1], op_v[(tp + T - i) % T, :, cols])
        mix_ref[:, cols] = acc.astype(BF16)

    @pl.loop(1, Pn)
    def _(d):
        b_copy(zi, d).wait_recv()

    shr[...] += dot(dwt[zi], ret[zi])

    @pl.loop(1, G)
    def _(i):
        g = (zi + i) % G
        p_arrival(g).wait_recv()
        shr[...] += prcv[g].astype(F32)

    moe_ref[...] = shr[...].astype(BF16)

    @pl.loop(0, G)
    def _(g):
        for way in (0, 1):
            @pl.when(z_sends(g, way))
            def _():
                m_copy(g, way).wait_send()
                z_copy(g, way).wait_send()

        @pl.when(g != zi)
        def _():
            p_copy(g).wait_send()

    @pl.loop(0, G)
    def _(r):
        @pl.loop(1, Pn)
        def _(d):
            b_copy(r, d).wait_send()

    @pl.loop(1, Pn)
    def _(d):
        d_copy(zi, d).wait_send()

    @pl.loop(1, E)
    def _(d):
        @pl.when(ep + d < E)
        def _():
            t_copy(d).wait_send()
            s_copy(d).wait_send()

    @pl.loop(1, T)
    def _(i):
        r_copy(i).wait_send()

    for da in range(A):
        if da:
            o1_copy(da, tp).wait_send()
            for dy in range(1, R):
                o2_copy(da, dy, yi).wait_send()
        for db in range(1, B):
            o3_copy(da, db, shard(da)).wait_send()


def local(
    query_rows, key_rows, value_rows, gate_rows, log_decay, out_proj,
    moe_input, norm_gain, routing, route_weight,
    expert_gate, expert_up, expert_down, shared_gate, shared_up, shared_down,
):
    E, T = lax.axis_size("ep"), lax.axis_size("tp")
    G = math.gcd(E, Z_GROUPS)
    Pn = (E // G) * T
    n = query_rows.shape[0]
    H = query_rows.shape[1] // DK
    nb = n // BLOCK
    tok, width = moe_input.shape
    visits = routing.shape[1]
    C = 2 * tok * visits // (E * T)
    ff = expert_gate.shape[2]
    assert shared_gate.shape[1] == ff
    rows_o = n // T
    dvl = H * DV

    cum = jnp.cumsum(log_decay.reshape(H, nb, BLOCK), axis=2)
    tot = jnp.sum(cum[:, :, -1], axis=1)
    tot = jnp.broadcast_to(jnp.pad(tot, (0, -H % 8))[:, None], (H + (-H % 8), 128))
    cum_b = cum.transpose(1, 0, 2)
    cum_c = cum.transpose(1, 2, 0)
    meta = jnp.concatenate([routing.T.astype(F32), route_weight.T], axis=0)

    vm = pl.BlockSpec(memory_space=pltpu.VMEM)
    hb = pl.BlockSpec(memory_space=pl.ANY)
    V = pltpu.VMEM
    dma = pltpu.SemaphoreType.DMA
    scratch = [
        V((n, H * DK), BF16), V((n, H * DK), BF16), V((n, dvl), BF16), V((n, dvl), BF16),
        V((T,) + out_proj.shape, BF16),
        V((width, ff), BF16), V((width, ff), BF16), V((ff, width), BF16),
        V((G, tok, width), BF16), V((G, 2 * visits, tok), F32),
        V((G, Pn * C, width), BF16), V((G, Pn * C, width), BF16), V((G, Pn * C, width), BF16),
        V((G, tok, Pn * C), BF16), V((tok, width), F32), V((G, tok, width), BF16),
        V((nb, H, DK, DV), F32), V((nb, H, DK, DV), BF16), V((H, DK, DV), BF16),
        V((E - 1, H, DK, DV), BF16), V((E,) + tot.shape, F32),
        V((T, rows_o, dvl), BF16), V((T - 1, rows_o, dvl), BF16), V((H, DK, DV), F32),
        dma((11,)),
        dma((2, G)), dma((G,)), dma((2, G)), dma((G,)),
        dma((G, Pn)), dma((G, Pn)), dma((G, Pn)), dma((G, Pn)),
        dma((G,)), dma((G,)),
        dma((E,)), dma((E,)), dma((E,)), dma((E,)),
        dma((T,)), dma((T,)), dma((T, E)), dma((T, E)), dma((T, T)), dma((T, T)),
        dma((T,)), dma((T,)),
    ]
    return pl.pallas_call(
        functools.partial(kernel, E, T, G, C),
        out_shape=(
            jax.ShapeDtypeStruct((rows_o, width), BF16),
            jax.ShapeDtypeStruct((tok, width), BF16),
        ),
        in_specs=[vm] * 6 + [hb] * 11,
        out_specs=(vm, vm),
        scratch_shapes=scratch,
        compiler_params=pltpu.CompilerParams(
            collective_id=0, has_side_effects=True, vmem_limit_bytes=67043328
        ),
        name="fused",
    )(
        moe_input, norm_gain[None, :], meta, cum_b, cum_c, tot,
        query_rows, key_rows, value_rows, gate_rows, out_proj,
        expert_gate, expert_up, expert_down, shared_gate, shared_up, shared_down,
    )


def solution(mesh):
    both = P(("ep", "tp"), None)
    in_specs = (
        P("ep", "tp"), P("ep", "tp"), P("ep", "tp"), P("ep", "tp"), P("tp", "ep"), P("tp", None),
        both, P(), both, both,
        P(("ep", "tp"), None, None), P(("ep", "tp"), None, None), P(("ep", "tp"), None, None),
        P(), P(), P(),
    )
    return jax.shard_map(
        local, mesh=mesh, in_specs=in_specs, out_specs=(both, both), check_vma=False
    )
```

profile of v0, /device:TPU:25, one launch (start us, length us, event | category | flops | bytes accessed | tf_op | source)
XLA Modules:
  0.0 173.3 jit_solution(3827343627730708154)
XLA Ops:
  0.6 0.7 convert_bitcast_fusion
  1.3 1.3 pad_maximum_fusion.meta_ref
  2.6 0.7 copy.23
  3.3 0.6 reduce_window_sum.11
  3.9 0.2 slice_reduce_fusion
  4.1 0.7 broadcast_in_dim.10.tot_ref
  4.7 0.6 copy.24
  5.3 1.3 copy.19
  6.7 162.6 %fused.1 = (bf16[512,2048]{1,0:T(8,128)(2,1)}, bf16[128,2048]{1,0:T(8,128)(2,1)}) custom-call(bf16[128,2048]{1,0:T(8,128)(2,1)} %x_ref.1, f32[1,2048]{1,0:T(1,128)} %bitcast.16, f32[8,128]{1,0:T(8,128)} %pad_maximum_fusion.meta_ref, f32[16,2,128]{2,1,0:T(2,128)} %bitcast.14, f32[16,128,2]{2,1,0:T(8,128)} %bitcast.12, f32[8,128]{1,0:T(8,128)} %broadcast_in_dim.10.tot_ref, ...), custom_call_target="tpu_custom_call" | custom-call | tf_op jit(solution)/shard_map/fused/pallas_call | solution.py:514
  169.3 0.0 copy-start
  169.3 3.2 %copy.27 = bf16[512,2048]{1,0:T(8,128)(2,1)} copy(bf16[512,2048]{1,0:T(8,128)(2,1)} %get-tuple-element.4) | data formatting | bytes 4194304
  172.5 0.0 copy-done
  172.5 0.8 copy.28
  (1 shorter events, 0.0 us)
Async XLA Ops:
  169.3 3.2 %copy-start = (bf16[128,2048]{1,0:T(8,128)(2,1)S(1)}, bf16[128,2048]{1,0:T(8,128)(2,1)}, u32[]{:S(2)}) copy-start(bf16[128,2048]{1,0:T(8,128)(2,1)} %get-tuple-element.5) | copy-start | bytes 1572868
where the time goes:
time: 174 us; the launch traced here: 173 us
  Pallas kernels  163 us (94%)
  local copies, waits for them, and re-layouts  7.37 us (4%)
  other arithmetic  2.7 us (2%)
    pallas_call x1, Pallas kernels, local(): pl.pallas_call(functools.partial(kernel, E, T, G, C), out_shape=(jax.Shap...  163 us
    unnamed x5, local copies, waits for them, and re-layouts  4.73 us

commit v1 on v0

--- a/solution.py
+++ b/solution.py
@@ -29,16 +29,17 @@
 
 def kernel(
     E, T, G, C,
-    x_ref, gain_ref, meta_ref, cum_ref, cumc_ref, tot_ref,
-    q_hbm, k_hbm, v_hbm, g_hbm, op_hbm,
+    gain_ref, route_ref, rweight_ref, decay_ref,
+    x_hbm, q_hbm, k_hbm, v_hbm, g_hbm, op_hbm,
     wg_hbm, wu_hbm, wd_hbm, sg_hbm, su_hbm, sd_hbm,
-    mix_ref, moe_ref,
+    mix_hbm, moe_hbm,
+    x_v, mix_v, moe_v, cum_ref, cumc_ref, tot_ref,
     q_v, k_v, v_v, g_v, op_v, wg_v, wu_v, wd_v,
     xz, mz, dsp, rcv, ret, dwt, shr, prcv,
     upd, sblk, lend, srcv, trcv, rs, rr, inc,
-    load_sem,
+    load_sem, mix_sem, moe_sem,
     z_s, z_r, m_s, m_r, d_s, d_r, b_s, b_r, p_s, p_r, s_s, s_r, t_s, t_r,
-    o1_s, o1_r, o2_s, o2_r, o3_s, o3_r, r_s, r_r,
+    o1_s, o1_r, o2_s, o2_r, o3_s, o3_r, oz_s, oz_r, r_s, r_r,
 ):
     ep = lax.axis_index("ep")
     tp = lax.axis_index("tp")
@@ -47,15 +48,17 @@
     zi = ep // R
     yi = ep % R
     j = yi * T + tp
-    tok, width = x_ref.shape
-    n_visits = meta_ref.shape[0] // 2
+    tok, width = x_v.shape
+    n_visits = route_ref.shape[0]
     nb = cum_ref.shape[0]
     H = cum_ref.shape[1]
     nbc = nb // T
     B = math.gcd(T, 2)
     A = T // B
     ta, tb = tp // B, tp % B
-    piece = op_v.shape[1] // R
+    Q = math.gcd(G, 2)
+    zq = zi % Q
+    piece = op_v.shape[1] // (R * Q)
     scale = DK ** (-0.5)
 
     loads = [
@@ -66,6 +69,8 @@
              (wu_hbm.at[0], wu_v), (wd_hbm.at[0], wd_v))
         )
     ]
+    x_load = pltpu.make_async_copy(x_hbm, x_v, load_sem.at[11])
+    x_load.start()
     for c in loads[:8]:
         c.start()
 
@@ -89,11 +94,13 @@
     def _(d):
         pl.semaphore_signal(barrier, inc=1, device_id=((ep + d) % E, tp), device_id_type=MESH)
 
-    xf = x_ref[...].astype(F32)
+    x_load.wait()
+    xf = x_v[...].astype(F32)
     xz[zi] = (
         xf * lax.rsqrt(jnp.mean(xf * xf, axis=-1, keepdims=True) + EPS) * gain_ref[...]
     ).astype(BF16)
-    mz[zi] = meta_ref[...]
+    mz[zi, 0:n_visits] = route_ref[...].astype(F32)
+    mz[zi, n_visits:2 * n_visits] = rweight_ref[...]
     pl.semaphore_wait(barrier, Pn - 1 + E - 1)
 
     def rcopy(src, dst, ss, rs_, dev):
@@ -145,23 +152,33 @@
     def shard(da, db=0):
         return ((ta + A - da) % A) * B + (tb + B - db) % B
 
-    def part(y):
-        return pl.ds(pl.multiple_of(y * piece, piece), piece)
+    def part(y, q):
+        return pl.ds(pl.multiple_of((q * R + y) * piece, piece), piece)
+
+    def half(q):
+        return pl.ds(pl.multiple_of(q * R * piece, R * piece), R * piece)
 
     def o1_copy(da, src):
-        at = op_v.at[src, part(yi)]
+        at = op_v.at[src, part(yi, zq)]
         return rcopy(at, at, o1_s.at[da], o1_r.at[da], (ep, ((ta + da) % A) * B + tb))
 
     def o2_copy(da, dy, y):
-        at = op_v.at[shard(da), part(y)]
+        at = op_v.at[shard(da), part(y, zq)]
         return rcopy(at, at, o2_s.at[da, dy], o2_r.at[da, dy], (zi * R + (yi + dy) % R, tp))
+
+    def oz_copy(da, dz, q):
+        at = op_v.at[shard(da), half(q)]
+        return rcopy(at, at, oz_s.at[da, dz], oz_r.at[da, dz],
+                     ((zi - zq + (zq + dz) % Q) * R + yi, tp))
 
     def o3_copy(da, db, src):
         at = op_v.at[src]
         return rcopy(at, at, o3_s.at[da, db], o3_r.at[da, db], (ep, ta * B + (tb + db) % B))
 
-    def r_copy(i):
-        return rcopy(rs.at[i], rr.at[i - 1], r_s.at[i], r_r.at[i], tp_peer(i))
+    def r_copy(da, db):
+        i = da * B + db
+        return rcopy(rs.at[i], rr.at[i - 1], r_s.at[i], r_r.at[i],
+                     (ep, ((ta + da) % A) * B + (tb + db) % B))
 
     for way in (0, 1):
         @pl.when(z_sends(zi, way))
@@ -202,8 +219,30 @@
 
     dispatch(zi)
 
+    blocks = jnp.concatenate(
+        [decay_ref[:, b * BLOCK:(b + 1) * BLOCK] for b in range(nb)], axis=0
+    )
+    upto = lax.broadcasted_iota(jnp.int32, (BLOCK, BLOCK), 0) <= lax.broadcasted_iota(
+        jnp.int32, (BLOCK, BLOCK), 1
+    )
+    cum = jnp.dot(
+        blocks, jnp.where(upto, 1.0, 0.0), precision=lax.Precision.HIGHEST,
+        preferred_element_type=F32,
+    )
+    cum_t = cum.T
+    for b in range(nb):
+        cum_ref[b] = cum[b * H:(b + 1) * H]
+        cumc_ref[b] = cum_t[:, b * H:(b + 1) * H]
+    tot_ref[...] = jnp.zeros_like(tot_ref)
+    tot_ref[0:H] = jnp.broadcast_to(
+        jnp.sum(decay_ref[...], axis=1, keepdims=True), (H, tot_ref.shape[1])
+    )
+
     loads[0].wait()
     loads[1].wait()
+
+    def state_rows(b, h):
+        return pl.ds(pl.multiple_of((b * H + h) * DK, DK), DK)
 
     inc[...] = jnp.zeros_like(inc)
 
@@ -220,7 +259,7 @@
                 u, v_v[rb, h * DV:(h + 1) * DV], (((0,), (0,)), ((), ())),
                 preferred_element_type=F32,
             )
-            upd[b, h] = add
+            upd[state_rows(b, h)] = add
             inc[h] = inc[h] * jnp.exp(last) + add
 
     lend[...] = inc[...].astype(BF16)
@@ -311,7 +350,7 @@
         for h in range(H):
             s = inc[h]
             sblk[b, h] = s.astype(BF16)
-            inc[h] = s * jnp.exp(crow[h:h + 1, BLOCK - 1:BLOCK]) + upd[b, h]
+            inc[h] = s * jnp.exp(crow[h:h + 1, BLOCK - 1:BLOCK]) + upd[state_rows(b, h)]
 
     loads[6].wait()
     loads[7].wait()
@@ -319,8 +358,8 @@
         jnp.int32, (BLOCK, BLOCK), 1
     )
 
-    def retain(i):
-        chunk = (tp + i) % T
+    def retain(i, da, db):
+        chunk = ((ta + da) % A) * B + (tb + db) % B
 
         @pl.loop(0, nbc)
         def _(w):
@@ -348,14 +387,12 @@
                 ).astype(BF16)
 
     @pl.loop(1, T)
-    def _(i):
-        retain(i)
-
-    retain(0)
-
-    @pl.loop(1, T)
-    def _(i):
-        r_copy(i).start()
+    def _(k):
+        i = T - k
+        retain(i, i // B, i % B)
+        r_copy(i // B, i % B).start()
+
+    retain(0, 0, 0)
 
     def combine(r):
         @pl.loop(1, Pn)
@@ -368,14 +405,6 @@
 
         dsp[r, 0:tok] = dot(dwt[r], ret[r]).astype(BF16)
         p_copy(r).start()
-
-    @pl.loop(1, 2 * G - 1)
-    def _(i):
-        g, there = group_at(i)
-
-        @pl.when(there)
-        def _():
-            combine(g)
 
     for da in range(1, A):
         o1_copy(da, shard(da)).wait_recv()
@@ -384,34 +413,53 @@
     for db in range(1, B):
         o3_copy(0, db, tp).start()
 
+    @pl.loop(1, 2 * G - 1)
+    def _(i):
+        g, there = group_at(i)
+
+        @pl.when(i == G - 1)
+        def _():
+            for da in range(1, A):
+                for dy in range(1, R):
+                    o2_copy(da, dy, (yi + R - dy) % R).wait_recv()
+                for dz in range(1, Q):
+                    oz_copy(da, dz, zq).start()
+
+        @pl.when(there)
+        def _():
+            combine(g)
+
     for da in range(1, A):
-        for dy in range(1, R):
-            o2_copy(da, dy, (yi + R - dy) % R).wait_recv()
+        for dz in range(1, Q):
+            oz_copy(da, dz, (zq + Q - dz) % Q).wait_recv()
         for db in range(1, B):
             o3_copy(da, db, shard(da)).start()
-
-    for da in range(A):
-        for db in range(1, B):
-            o3_copy(da, db, shard(da, db)).wait_recv()
-
-    @pl.loop(1, T)
-    def _(i):
-        r_copy(i).wait_recv()
-
-    n_col = 512
-    @pl.loop(0, width // n_col)
-    def _(n):
-        cols = pl.ds(pl.multiple_of(n * n_col, n_col), n_col)
-        acc = dot(rs[0], op_v[tp, :, cols])
-        for i in range(1, T):
-            acc += dot(rr[i - 1], op_v[(tp + T - i) % T, :, cols])
-        mix_ref[:, cols] = acc.astype(BF16)
 
     @pl.loop(1, Pn)
     def _(d):
         b_copy(zi, d).wait_recv()
 
     shr[...] += dot(dwt[zi], ret[zi])
+
+    for db in range(1, B):
+        o3_copy(0, db, shard(0, db)).wait_recv()
+        r_copy(0, db).wait_recv()
+
+    n_col = upd.shape[1]
+    n_out = width // n_col
+
+    def columns(n):
+        return pl.ds(pl.multiple_of(n * n_col, n_col), n_col)
+
+    def out_rows(n):
+        return pl.ds(pl.multiple_of(n * mix_v.shape[0], mix_v.shape[0]), mix_v.shape[0])
+
+    @pl.loop(0, n_out)
+    def _(n):
+        acc = dot(rs[0], op_v[tp, :, columns(n)])
+        for db in range(1, B):
+            acc += dot(rr[db - 1], op_v[shard(0, db), :, columns(n)])
+        upd[out_rows(n)] = acc
 
     @pl.loop(1, G)
     def _(i):
@@ -419,7 +467,29 @@
         p_arrival(g).wait_recv()
         shr[...] += prcv[g].astype(F32)
 
-    moe_ref[...] = shr[...].astype(BF16)
+    moe_v[...] = shr[...].astype(BF16)
+    moe_out = pltpu.make_async_copy(moe_v, moe_hbm, moe_sem)
+    moe_out.start()
+
+    for da in range(1, A):
+        for db in range(B):
+            if db:
+                o3_copy(da, db, shard(da, db)).wait_recv()
+            r_copy(da, db).wait_recv()
+
+    def mix_out(n):
+        return pltpu.make_async_copy(
+            mix_v.at[:, columns(n)], mix_hbm.at[:, columns(n)], mix_sem.at[n]
+        )
+
+    @pl.loop(0, n_out)
+    def _(n):
+        acc = upd[out_rows(n)]
+        for da in range(1, A):
+            for db in range(B):
+                acc += dot(rr[da * B + db - 1], op_v[shard(da, db), :, columns(n)])
+        mix_v[:, columns(n)] = acc.astype(BF16)
+        mix_out(n).start()
 
     @pl.loop(0, G)
     def _(g):
@@ -450,17 +520,26 @@
             t_copy(d).wait_send()
             s_copy(d).wait_send()
 
-    @pl.loop(1, T)
-    def _(i):
-        r_copy(i).wait_send()
+    for da in range(A):
+        for db in range(B):
+            if da or db:
+                r_copy(da, db).wait_send()
 
     for da in range(A):
         if da:
             o1_copy(da, tp).wait_send()
             for dy in range(1, R):
                 o2_copy(da, dy, yi).wait_send()
+            for dz in range(1, Q):
+                oz_copy(da, dz, zq).wait_send()
         for db in range(1, B):
             o3_copy(da, db, shard(da)).wait_send()
+
+    moe_out.wait()
+
+    @pl.loop(0, n_out)
+    def _(n):
+        mix_out(n).wait()
 
 
 def local(
@@ -482,33 +561,30 @@
     rows_o = n // T
     dvl = H * DV
 
-    cum = jnp.cumsum(log_decay.reshape(H, nb, BLOCK), axis=2)
-    tot = jnp.sum(cum[:, :, -1], axis=1)
-    tot = jnp.broadcast_to(jnp.pad(tot, (0, -H % 8))[:, None], (H + (-H % 8), 128))
-    cum_b = cum.transpose(1, 0, 2)
-    cum_c = cum.transpose(1, 2, 0)
-    meta = jnp.concatenate([routing.T.astype(F32), route_weight.T], axis=0)
-
     vm = pl.BlockSpec(memory_space=pltpu.VMEM)
     hb = pl.BlockSpec(memory_space=pl.ANY)
     V = pltpu.VMEM
     dma = pltpu.SemaphoreType.DMA
+    rows_t = H + (-H % 8)
     scratch = [
+        V((tok, width), BF16), V((rows_o, width), BF16), V((tok, width), BF16),
+        V((nb, H, BLOCK), F32), V((nb, BLOCK, H), F32), V((rows_t, 128), F32),
         V((n, H * DK), BF16), V((n, H * DK), BF16), V((n, dvl), BF16), V((n, dvl), BF16),
         V((T,) + out_proj.shape, BF16),
         V((width, ff), BF16), V((width, ff), BF16), V((ff, width), BF16),
         V((G, tok, width), BF16), V((G, 2 * visits, tok), F32),
         V((G, Pn * C, width), BF16), V((G, Pn * C, width), BF16), V((G, Pn * C, width), BF16),
         V((G, tok, Pn * C), BF16), V((tok, width), F32), V((G, tok, width), BF16),
-        V((nb, H, DK, DV), F32), V((nb, H, DK, DV), BF16), V((H, DK, DV), BF16),
-        V((E - 1, H, DK, DV), BF16), V((E,) + tot.shape, F32),
+        V((max(nb * H * DK, rows_o * width // DV), DV), F32), V((nb, H, DK, DV), BF16), V((H, DK, DV), BF16),
+        V((E - 1, H, DK, DV), BF16), V((E, rows_t, 128), F32),
         V((T, rows_o, dvl), BF16), V((T - 1, rows_o, dvl), BF16), V((H, DK, DV), F32),
-        dma((11,)),
+        dma((12,)), dma((width // DV,)), dma,
         dma((2, G)), dma((G,)), dma((2, G)), dma((G,)),
         dma((G, Pn)), dma((G, Pn)), dma((G, Pn)), dma((G, Pn)),
         dma((G,)), dma((G,)),
         dma((E,)), dma((E,)), dma((E,)), dma((E,)),
         dma((T,)), dma((T,)), dma((T, E)), dma((T, E)), dma((T, T)), dma((T, T)),
+        dma((T, G)), dma((T, G)),
         dma((T,)), dma((T,)),
     ]
     return pl.pallas_call(
@@ -517,16 +593,16 @@
             jax.ShapeDtypeStruct((rows_o, width), BF16),
             jax.ShapeDtypeStruct((tok, width), BF16),
         ),
-        in_specs=[vm] * 6 + [hb] * 11,
-        out_specs=(vm, vm),
+        in_specs=[vm] * 4 + [hb] * 12,
+        out_specs=(hb, hb),
         scratch_shapes=scratch,
         compiler_params=pltpu.CompilerParams(
             collective_id=0, has_side_effects=True, vmem_limit_bytes=67043328
         ),
         name="fused",
     )(
-        moe_input, norm_gain[None, :], meta, cum_b, cum_c, tot,
-        query_rows, key_rows, value_rows, gate_rows, out_proj,
+        norm_gain[None, :], routing.T, route_weight.T, log_decay,
+        moe_input, query_rows, key_rows, value_rows, gate_rows, out_proj,
         expert_gate, expert_up, expert_down, shared_gate, shared_up, shared_down,
     )
 

time: 174 us -> 187 us (1.075)
  the two profiles are of different devices: /device:TPU:25 before, /device:TPU:2 now
where the time goes in v1:
time: 187 us; the launch traced here: 184 us
  Pallas kernels  179 us (96%)
  local copies, waits for them, and re-layouts  4.01 us (2%)
    pallas_call x1, Pallas kernels, local(): pl.pallas_call(functools.partial(kernel, E, T, G, C), out_shape=(jax.Shap...  179 us
    unnamed x4, local copies, waits for them, and re-layouts  4.01 us

profile of v1, /device:TPU:2, one launch (start us, length us, event | category | flops | bytes accessed | tf_op | source)
XLA Modules:
  0.0 183.7 jit_solution(13615007750270431434)
XLA Ops:
  0.6 179.0 %fused.1 = (bf16[512,2048]{1,0:T(8,128)(2,1)}, bf16[128,2048]{1,0:T(8,128)(2,1)}) custom-call(f32[1,2048]{1,0:T(1,128)} %bitcast.3, s32[4,128]{1,0:T(4,128)} %bitcast.4, f32[4,128]{1,0:T(4,128)} %bitcast.5, f32[2,2048]{1,0:T(2,128)} %decay_ref.1, bf16[128,2048]{1,0:T(8,128)(2,1)} %x_hbm.1, bf16[2048,256]{1,0:T(8,128)(2,1)} %q_hbm.1, ...), custom_call_target="tpu_custom_call" | custom-call | tf_op jit(solution)/shard_map/fused/pallas_call | solution.py:590
  179.7 0.0 copy-start
  179.7 3.2 %copy.20 = bf16[512,2048]{1,0:T(8,128)(2,1)} copy(bf16[512,2048]{1,0:T(8,128)(2,1)} %get-tuple-element.4) | data formatting | bytes 4194304
  182.9 0.0 copy-done
  182.9 0.8 copy.21
Async XLA Ops:
  179.7 3.2 %copy-start = (bf16[128,2048]{1,0:T(8,128)(2,1)S(1)}, bf16[128,2048]{1,0:T(8,128)(2,1)}, u32[]{:S(2)}) copy-start(bf16[128,2048]{1,0:T(8,128)(2,1)} %get-tuple-element.5) | copy-start | bytes 1572868

commit v2 on v1

--- a/solution.py
+++ b/solution.py
@@ -33,12 +33,12 @@
     x_hbm, q_hbm, k_hbm, v_hbm, g_hbm, op_hbm,
     wg_hbm, wu_hbm, wd_hbm, sg_hbm, su_hbm, sd_hbm,
     mix_hbm, moe_hbm,
-    x_v, mix_v, moe_v, cum_ref, cumc_ref, tot_ref,
+    x_v, mix_v, moe_v, cum_ref, cumc_ref,
     q_v, k_v, v_v, g_v, op_v, wg_v, wu_v, wd_v,
     xz, mz, dsp, rcv, ret, dwt, shr, prcv,
-    upd, sblk, lend, srcv, trcv, rs, rr, inc,
+    upd, sblk, srcv, trcv, zrcv, ztot, pre, rs, rr, inc,
     load_sem, mix_sem, moe_sem,
-    z_s, z_r, m_s, m_r, d_s, d_r, b_s, b_r, p_s, p_r, s_s, s_r, t_s, t_r,
+    z_s, z_r, m_s, m_r, d_s, d_r, b_s, b_r, p_s, p_r, s_s, s_r, t_s, t_r, e_s, e_r, f_s, f_r,
     o1_s, o1_r, o2_s, o2_r, o3_s, o3_r, oz_s, oz_r, r_s, r_r,
 ):
     ep = lax.axis_index("ep")
@@ -121,21 +121,29 @@
             return (g <= zi) & (zi + 1 < G)
         return (g >= zi) & (zi > 0)
 
-    def group_at(i):
-        dist = (i + 1) // 2
-        g = zi + jnp.where(i % 2 == 1, -dist, dist)
-        return g, (g >= 0) & (g < G)
+    def nth(n):
+        m = jnp.minimum(zi, G - 1 - zi)
+        near = zi + (n // 2 if n % 2 == 0 else -((n + 1) // 2))
+        far = zi + jnp.where(2 * zi > G - 1, m - n, n - m)
+        return jnp.where(n <= 2 * m, near, far)
 
     def rows(d):
         return pl.ds(pl.multiple_of(d * C, C), C)
 
     def d_copy(r, d):
-        return rcopy(dsp.at[r, rows(d)], rcv.at[r, rows(d)], d_s.at[r, d], d_r.at[r, d],
-                     plane_peer(d))
+        return rcopy(dsp.at[r, rows(d)], rcv.at[r, rows(d)], d_s.at[r], d_r.at[r], plane_peer(d))
 
     def b_copy(r, d):
-        return rcopy(rcv.at[r, rows(d)], ret.at[r, rows(d)], b_s.at[r, d], b_r.at[r, d],
+        return rcopy(rcv.at[r, rows(d)], ret.at[r, rows(d)], b_s.at[r], b_r.at[r],
                      plane_peer(Pn - d))
+
+    others = pl.ds(C, (Pn - 1) * C)
+
+    def d_all(r):
+        return rcopy(dsp.at[r, others], rcv.at[r, others], d_s.at[r], d_r.at[r], plane_peer(1))
+
+    def b_all(r):
+        return rcopy(rcv.at[r, others], ret.at[r, others], b_s.at[r], b_r.at[r], plane_peer(1))
 
     def p_copy(g):
         return rcopy(dsp.at[g, 0:tok], prcv.at[zi], p_s.at[g], p_r.at[zi], z_place(g))
@@ -144,10 +152,18 @@
         return rcopy(dsp.at[g, 0:tok], prcv.at[g], p_s.at[g], p_r.at[g], z_place(g))
 
     def s_copy(d):
-        return rcopy(lend, srcv.at[d - 1], s_s.at[d], s_r.at[d], ((ep + d) % E, tp))
+        return rcopy(srcv.at[0], srcv.at[d], s_s.at[d], s_r.at[d],
+                     (zi * R + (yi + d) % R, tp))
 
     def t_copy(d):
-        return rcopy(tot_ref, trcv.at[d], t_s.at[d], t_r.at[d], ((ep + d) % E, tp))
+        return rcopy(trcv.at[0], trcv.at[d], t_s.at[d], t_r.at[d],
+                     (zi * R + (yi + d) % R, tp))
+
+    def e_copy(d):
+        return rcopy(zrcv.at[0], zrcv.at[d], e_s.at[d], e_r.at[d], z_place((zi + d) % G))
+
+    def f_copy(d):
+        return rcopy(ztot.at[0], ztot.at[d], f_s.at[d], f_r.at[d], z_place((zi + d) % G))
 
     def shard(da, db=0):
         return ((ta + A - da) % A) * B + (tb + B - db) % B
@@ -233,9 +249,9 @@
     for b in range(nb):
         cum_ref[b] = cum[b * H:(b + 1) * H]
         cumc_ref[b] = cum_t[:, b * H:(b + 1) * H]
-    tot_ref[...] = jnp.zeros_like(tot_ref)
-    tot_ref[0:H] = jnp.broadcast_to(
-        jnp.sum(decay_ref[...], axis=1, keepdims=True), (H, tot_ref.shape[1])
+    trcv[0] = jnp.zeros_like(trcv[0])
+    trcv[0, 0:H] = jnp.broadcast_to(
+        jnp.sum(decay_ref[...], axis=1, keepdims=True), (H, trcv.shape[2])
     )
 
     loads[0].wait()
@@ -262,7 +278,12 @@
             upd[state_rows(b, h)] = add
             inc[h] = inc[h] * jnp.exp(last) + add
 
-    lend[...] = inc[...].astype(BF16)
+    srcv[0] = inc[...].astype(BF16)
+
+    @pl.loop(1, R)
+    def _(d):
+        t_copy(d).start()
+        s_copy(d).start()
 
     loads[3].wait()
     loads[4].wait()
@@ -273,10 +294,7 @@
         c.start()
 
     def serve(r):
-        @pl.loop(1, Pn)
-        def _(d):
-            d_copy(r, d).wait_recv()
-
+        d_all(r).wait_recv()
         rows_in = rcv[r]
         hidden = (silu(dot(rows_in, wg_v[...])) * dot(rows_in, wu_v[...])).astype(BF16)
         res = dot(hidden, wd_v[...]).astype(BF16)
@@ -287,73 +305,77 @@
         def _(d):
             b_copy(r, d).start()
 
-    loads[8].wait()
-    loads[9].wait()
-    loads[10].wait()
-    @pl.loop(1, 2 * G - 1)
-    def _(i):
-        g, there = group_at(i)
-
-        @pl.when(there)
-        def _():
-            m_copy(g, 0).wait_recv()
-            z_copy(g, 0).wait_recv()
-            for way in (0, 1):
-                @pl.when(z_sends(g, way))
-                def _():
-                    m_copy(g, way).start()
-                    z_copy(g, way).start()
-            dispatch(g)
-
-        @pl.when(i == G - 1)
-        def _():
-            @pl.loop(1, E)
-            def _(d):
-                @pl.when(ep + d < E)
-                def _():
-                    t_copy(d).start()
-                    s_copy(d).start()
-
-        behind, known = group_at(i - 2)
-
-        @pl.when(known & (i >= 2))
-        def _():
-            serve(behind)
-
-    loads[2].wait()
-    for da in range(1, A):
-        o1_copy(da, tp).start()
-    for i in (2 * G - 3, 2 * G - 2):
-        g, there = group_at(jnp.int32(i))
-
-        @pl.when(there)
-        def _():
-            serve(g)
-
-    inc[...] = jnp.zeros_like(inc)
-
-    @pl.loop(1, E)
-    def _(i):
-        d = E - i
-
-        @pl.when(ep >= d)
-        def _():
+    def arrive(g):
+        m_copy(g, 0).wait_recv()
+        z_copy(g, 0).wait_recv()
+        for way in (0, 1):
+            @pl.when(z_sends(g, way))
+            def _():
+                m_copy(g, way).start()
+                z_copy(g, way).start()
+        dispatch(g)
+
+    def plane_state():
+        inc[...] = jnp.zeros_like(inc)
+        ztot[0] = trcv[0]
+
+        @pl.loop(1, R)
+        def _(d):
             t_copy(d).wait_recv()
             s_copy(d).wait_recv()
+            ztot[0] += trcv[d]
+
+        @pl.loop(0, R)
+        def _(y):
+            d = (yi + R - y) % R
+
+            @pl.when(y == yi)
+            def _():
+                pre[...] = inc[...]
+
             for h in range(H):
-                shrink = jnp.exp(trcv[d, h:h + 1, 0:1])
-                inc[h] = inc[h] * shrink + srcv[d - 1, h].astype(F32)
-
-    @pl.loop(0, nb)
-    def _(b):
-        crow = cum_ref[b]
-        for h in range(H):
-            s = inc[h]
-            sblk[b, h] = s.astype(BF16)
-            inc[h] = s * jnp.exp(crow[h:h + 1, BLOCK - 1:BLOCK]) + upd[state_rows(b, h)]
-
-    loads[6].wait()
-    loads[7].wait()
+                inc[h] = inc[h] * jnp.exp(trcv[d, h:h + 1, 0:1]) + srcv[d, h].astype(F32)
+
+        zrcv[0] = inc[...].astype(BF16)
+
+        @pl.loop(1, G)
+        def _(d):
+            @pl.when(zi + d < G)
+            def _():
+                f_copy(d).start()
+                e_copy(d).start()
+
+    def carried_state():
+        inc[...] = jnp.zeros_like(inc)
+
+        @pl.loop(1, G)
+        def _(i):
+            d = G - i
+
+            @pl.when(zi >= d)
+            def _():
+                f_copy(d).wait_recv()
+                e_copy(d).wait_recv()
+                for h in range(H):
+                    inc[h] = inc[h] * jnp.exp(ztot[d, h:h + 1, 0:1]) + zrcv[d, h].astype(F32)
+
+        @pl.loop(0, R)
+        def _(y):
+            @pl.when(y < yi)
+            def _():
+                for h in range(H):
+                    inc[h] = inc[h] * jnp.exp(trcv[(yi + R - y) % R, h:h + 1, 0:1])
+
+        inc[...] += pre[...]
+
+        @pl.loop(0, nb)
+        def _(b):
+            crow = cum_ref[b]
+            for h in range(H):
+                s = inc[h]
+                sblk[b, h] = s.astype(BF16)
+                inc[h] = s * jnp.exp(crow[h:h + 1, BLOCK - 1:BLOCK]) + upd[state_rows(b, h)]
+
     causal = lax.broadcasted_iota(jnp.int32, (BLOCK, BLOCK), 0) >= lax.broadcasted_iota(
         jnp.int32, (BLOCK, BLOCK), 1
     )
@@ -386,59 +408,62 @@
                     silu(gate) * (cen * lax.rsqrt(var + EPS))
                 ).astype(BF16)
 
-    @pl.loop(1, T)
-    def _(k):
-        i = T - k
-        retain(i, i // B, i % B)
-        r_copy(i // B, i % B).start()
-
-    retain(0, 0, 0)
-
     def combine(r):
-        @pl.loop(1, Pn)
-        def _(d):
-            b_copy(r, d).wait_recv()
-
-        @pl.loop(1, Pn)
-        def _(d):
-            d_copy(r, d).wait_send()
-
+        b_all(r).wait_recv()
+        d_all(r).wait_send()
         dsp[r, 0:tok] = dot(dwt[r], ret[r]).astype(BF16)
         p_copy(r).start()
 
+    near = [nth(n) for n in range(1, G)]
+    for c in loads[8:]:
+        c.wait()
+    arrive(near[0])
+    loads[2].wait()
+    for da in range(1, A):
+        o1_copy(da, tp).start()
+    for db in range(1, B):
+        o3_copy(0, db, tp).start()
+    plane_state()
+    arrive(near[1])
+    serve(near[0])
     for da in range(1, A):
         o1_copy(da, shard(da)).wait_recv()
         for dy in range(1, R):
             o2_copy(da, dy, yi).start()
+    for g in near[2:]:
+        arrive(g)
+    carried_state()
+    loads[6].wait()
+    loads[7].wait()
+
+    @pl.loop(0, T)
+    def _(i):
+        retain(i, i // B, i % B)
+    serve(near[1])
+    for da in range(1, A):
+        for dy in range(1, R):
+            o2_copy(da, dy, (yi + R - dy) % R).wait_recv()
+        for dz in range(1, Q):
+            oz_copy(da, dz, zq).start()
+    combine(near[0])
+    for g in near[2:]:
+        serve(g)
+    serve(zi)
+    for da in range(1, A):
+        for db in range(B):
+            r_copy(da, db).start()
     for db in range(1, B):
-        o3_copy(0, db, tp).start()
-
-    @pl.loop(1, 2 * G - 1)
-    def _(i):
-        g, there = group_at(i)
-
-        @pl.when(i == G - 1)
-        def _():
-            for da in range(1, A):
-                for dy in range(1, R):
-                    o2_copy(da, dy, (yi + R - dy) % R).wait_recv()
-                for dz in range(1, Q):
-                    oz_copy(da, dz, zq).start()
-
-        @pl.when(there)
-        def _():
-            combine(g)
-
+        r_copy(0, db).start()
+    combine(near[1])
+    for g in near[2:]:
+        combine(g)
     for da in range(1, A):
         for dz in range(1, Q):
             oz_copy(da, dz, (zq + Q - dz) % Q).wait_recv()
         for db in range(1, B):
             o3_copy(da, db, shard(da)).start()
 
-    @pl.loop(1, Pn)
-    def _(d):
-        b_copy(zi, d).wait_recv()
-
+    b_all(zi).wait_recv()
     shr[...] += dot(dwt[zi], ret[zi])
 
     for db in range(1, B):
@@ -471,25 +496,27 @@
     moe_out = pltpu.make_async_copy(moe_v, moe_hbm, moe_sem)
     moe_out.start()
 
+    def mix_out(n):
+        return pltpu.make_async_copy(
+            mix_v.at[:, columns(n)], mix_hbm.at[:, columns(n)], mix_sem.at[n]
+        )
+
     for da in range(1, A):
         for db in range(B):
             if db:
                 o3_copy(da, db, shard(da, db)).wait_recv()
             r_copy(da, db).wait_recv()
 
-    def mix_out(n):
-        return pltpu.make_async_copy(
-            mix_v.at[:, columns(n)], mix_hbm.at[:, columns(n)], mix_sem.at[n]
-        )
-
-    @pl.loop(0, n_out)
-    def _(n):
-        acc = upd[out_rows(n)]
-        for da in range(1, A):
-            for db in range(B):
-                acc += dot(rr[da * B + db - 1], op_v[shard(da, db), :, columns(n)])
-        mix_v[:, columns(n)] = acc.astype(BF16)
-        mix_out(n).start()
+            @pl.loop(0, n_out)
+            def _(n):
+                acc = upd[out_rows(n)] + dot(
+                    rr[da * B + db - 1], op_v[shard(da, db), :, columns(n)]
+                )
+                if da == A - 1 and db == B - 1:
+                    mix_v[:, columns(n)] = acc.astype(BF16)
+                    mix_out(n).start()
+                else:
+                    upd[out_rows(n)] = acc
 
     @pl.loop(0, G)
     def _(g):
@@ -505,20 +532,21 @@
 
     @pl.loop(0, G)
     def _(r):
-        @pl.loop(1, Pn)
-        def _(d):
-            b_copy(r, d).wait_send()
-
-    @pl.loop(1, Pn)
+        b_all(r).wait_send()
+
+    d_all(zi).wait_send()
+
+    @pl.loop(1, R)
     def _(d):
-        d_copy(zi, d).wait_send()
-
-    @pl.loop(1, E)
+        t_copy(d).wait_send()
+        s_copy(d).wait_send()
+
+    @pl.loop(1, G)
     def _(d):
-        @pl.when(ep + d < E)
+        @pl.when(zi + d < G)
         def _():
-            t_copy(d).wait_send()
-            s_copy(d).wait_send()
+            f_copy(d).wait_send()
+            e_copy(d).wait_send()
 
     for da in range(A):
         for db in range(B):
@@ -549,7 +577,11 @@
 ):
     E, T = lax.axis_size("ep"), lax.axis_size("tp")
     G = math.gcd(E, Z_GROUPS)
-    Pn = (E // G) * T
+    R = E // G
+    Pn = R * T
+    B = math.gcd(T, 2)
+    A = T // B
+    Q = math.gcd(G, 2)
     n = query_rows.shape[0]
     H = query_rows.shape[1] // DK
     nb = n // BLOCK
@@ -568,24 +600,24 @@
     rows_t = H + (-H % 8)
     scratch = [
         V((tok, width), BF16), V((rows_o, width), BF16), V((tok, width), BF16),
-        V((nb, H, BLOCK), F32), V((nb, BLOCK, H), F32), V((rows_t, 128), F32),
+        V((nb, H, BLOCK), F32), V((nb, BLOCK, H), F32),
         V((n, H * DK), BF16), V((n, H * DK), BF16), V((n, dvl), BF16), V((n, dvl), BF16),
         V((T,) + out_proj.shape, BF16),
         V((width, ff), BF16), V((width, ff), BF16), V((ff, width), BF16),
         V((G, tok, width), BF16), V((G, 2 * visits, tok), F32),
         V((G, Pn * C, width), BF16), V((G, Pn * C, width), BF16), V((G, Pn * C, width), BF16),
         V((G, tok, Pn * C), BF16), V((tok, width), F32), V((G, tok, width), BF16),
-        V((max(nb * H * DK, rows_o * width // DV), DV), F32), V((nb, H, DK, DV), BF16), V((H, DK, DV), BF16),
-        V((E - 1, H, DK, DV), BF16), V((E, rows_t, 128), F32),
+        V((max(nb * H * DK, rows_o * width // DV), DV), F32), V((nb, H, DK, DV), BF16),
+        V((R, H, DK, DV), BF16), V((R, rows_t, 128), F32),
+        V((G, H, DK, DV), BF16), V((G, rows_t, 128), F32), V((H, DK, DV), F32),
         V((T, rows_o, dvl), BF16), V((T - 1, rows_o, dvl), BF16), V((H, DK, DV), F32),
         dma((12,)), dma((width // DV,)), dma,
         dma((2, G)), dma((G,)), dma((2, G)), dma((G,)),
-        dma((G, Pn)), dma((G, Pn)), dma((G, Pn)), dma((G, Pn)),
+        dma((G,)), dma((G,)), dma((G,)), dma((G,)),
         dma((G,)), dma((G,)),
-        dma((E,)), dma((E,)), dma((E,)), dma((E,)),
-        dma((T,)), dma((T,)), dma((T, E)), dma((T, E)), dma((T, T)), dma((T, T)),
-        dma((T, G)), dma((T, G)),
-        dma((T,)), dma((T,)),
+        dma((R,)), dma((R,)), dma((R,)), dma((R,)), dma((G,)), dma((G,)), dma((G,)), dma((G,)),
+        dma((A,)), dma((A,)), dma((A, R)), dma((A, R)), dma((A, B)), dma((A, B)),
+        dma((A, Q)), dma((A, Q)), dma((T,)), dma((T,)),
     ]
     return pl.pallas_call(
         functools.partial(kernel, E, T, G, C),

time: 187 us -> 149 us (0.80)
  Pallas kernels: 179 us -> 143 us
    pallas_call x1, Pallas kernels: 179 us -> 143 us  [local(): pl.pallas_call(functools.partial(kernel, E, T, G, C), out_shape=(jax.Shap...]
where the time goes in v2:
time: 149 us; the launch traced here: 147 us
  Pallas kernels  143 us (96%)
  local copies, waits for them, and re-layouts  4.01 us (3%)
    pallas_call x1, Pallas kernels, local(): pl.pallas_call(functools.partial(kernel, E, T, G, C), out_shape=(jax.Shap...  143 us
    unnamed x4, local copies, waits for them, and re-layouts  4.01 us

profile of v2, /device:TPU:2, one launch (start us, length us, event | category | flops | bytes accessed | tf_op | source)
XLA Modules:
  0.0 147.2 jit_solution(15342756832867302012)
XLA Ops:
  0.6 142.6 %fused.1 = (bf16[512,2048]{1,0:T(8,128)(2,1)}, bf16[128,2048]{1,0:T(8,128)(2,1)}) custom-call(f32[1,2048]{1,0:T(1,128)} %bitcast.3, s32[4,128]{1,0:T(4,128)} %bitcast.4, f32[4,128]{1,0:T(4,128)} %bitcast.5, f32[2,2048]{1,0:T(2,128)} %decay_ref.1, bf16[128,2048]{1,0:T(8,128)(2,1)} %x_hbm.1, bf16[2048,256]{1,0:T(8,128)(2,1)} %q_hbm.1, ...), custom_call_target="tpu_custom_call" | custom-call | tf_op jit(solution)/shard_map/fused/pallas_call | solution.py:622
  143.2 0.0 copy-start
  143.2 3.2 %copy.20 = bf16[512,2048]{1,0:T(8,128)(2,1)} copy(bf16[512,2048]{1,0:T(8,128)(2,1)} %get-tuple-element.4) | data formatting | bytes 4194304
  146.4 0.0 copy-done
  146.4 0.8 copy.21
Async XLA Ops:
  143.2 3.2 %copy-start = (bf16[128,2048]{1,0:T(8,128)(2,1)S(1)}, bf16[128,2048]{1,0:T(8,128)(2,1)}, u32[]{:S(2)}) copy-start(bf16[128,2048]{1,0:T(8,128)(2,1)} %get-tuple-element.5) | copy-start | bytes 1572868

commit v3 on v2

--- a/solution.py
+++ b/solution.py
@@ -56,9 +56,7 @@
     B = math.gcd(T, 2)
     A = T // B
     ta, tb = tp // B, tp % B
-    Q = math.gcd(G, 2)
-    zq = zi % Q
-    piece = op_v.shape[1] // (R * Q)
+    piece = op_v.shape[1] // E
     scale = DK ** (-0.5)
 
     loads = [
@@ -81,9 +79,6 @@
         p = (j + d) % Pn
         return (zi * R + p // T, p % T)
 
-    def tp_peer(i):
-        return (ep, (tp + i) % T)
-
     barrier = pltpu.get_barrier_semaphore()
 
     @pl.loop(1, Pn)
@@ -123,9 +118,9 @@
 
     def nth(n):
         m = jnp.minimum(zi, G - 1 - zi)
-        near = zi + (n // 2 if n % 2 == 0 else -((n + 1) // 2))
+        step = (2 * (zi % 2) - 1) * (2 * (n % 2) - 1)
         far = zi + jnp.where(2 * zi > G - 1, m - n, n - m)
-        return jnp.where(n <= 2 * m, near, far)
+        return jnp.where(n <= 2 * m, zi + step * ((n + 1) // 2), far)
 
     def rows(d):
         return pl.ds(pl.multiple_of(d * C, C), C)
@@ -168,32 +163,48 @@
     def shard(da, db=0):
         return ((ta + A - da) % A) * B + (tb + B - db) % B
 
-    def part(y, q):
-        return pl.ds(pl.multiple_of((q * R + y) * piece, piece), piece)
-
-    def half(q):
-        return pl.ds(pl.multiple_of(q * R * piece, R * piece), R * piece)
+    def part(y):
+        return pl.ds(pl.multiple_of((zi * R + y) * piece, piece), piece)
 
     def o1_copy(da, src):
-        at = op_v.at[src, part(yi, zq)]
+        at = op_v.at[src, part(yi)]
         return rcopy(at, at, o1_s.at[da], o1_r.at[da], (ep, ((ta + da) % A) * B + tb))
 
     def o2_copy(da, dy, y):
-        at = op_v.at[shard(da), part(y, zq)]
+        at = op_v.at[shard(da), part(y)]
         return rcopy(at, at, o2_s.at[da, dy], o2_r.at[da, dy], (zi * R + (yi + dy) % R, tp))
 
-    def oz_copy(da, dz, q):
-        at = op_v.at[shard(da), half(q)]
-        return rcopy(at, at, oz_s.at[da, dz], oz_r.at[da, dz],
-                     ((zi - zq + (zq + dz) % Q) * R + yi, tp))
+    def oz_copy(da, g, way):
+        to = (zi - 1, zi + 1)[way]
+        at = op_v.at[shard(da), pl.ds(pl.multiple_of(g * R * piece, R * piece), R * piece)]
+        return rcopy(at, at, oz_s.at[da, way, g], oz_r.at[da, g], z_place(to))
+
+    def oz_sends(g):
+        for da in range(1, A):
+            for way in (0, 1):
+                @pl.when(z_sends(g, way))
+                def _():
+                    oz_copy(da, g, way).start()
+
+    def oz_receive(g):
+        for da in range(1, A):
+            oz_copy(da, g, 0).wait_recv()
+        oz_sends(g)
 
     def o3_copy(da, db, src):
         at = op_v.at[src]
         return rcopy(at, at, o3_s.at[da, db], o3_r.at[da, db], (ep, ta * B + (tb + db) % B))
 
-    def r_copy(da, db):
+    halves = 1
+    strip = mix_v.shape[0] // halves
+
+    def strip_of(part):
+        return slice(part * strip, (part + 1) * strip)
+
+    def r_copy(da, db, part):
         i = da * B + db
-        return rcopy(rs.at[i], rr.at[i - 1], r_s.at[i], r_r.at[i],
+        return rcopy(rs.at[i, strip_of(w)], rr.at[i - 1, strip_of(w)],
+                     r_s.at[i, part], r_r.at[i, part],
                      (ep, ((ta + da) % A) * B + (tb + db) % B))
 
     for way in (0, 1):
@@ -233,6 +244,10 @@
         def _(d):
             d_copy(r, d).start()
 
+    loads[2].wait()
+    for da in range(1, A):
+        o1_copy(da, tp).start()
+
     dispatch(zi)
 
     blocks = jnp.concatenate(
@@ -305,7 +320,7 @@
         def _(d):
             b_copy(r, d).start()
 
-    def arrive(g):
+    def receive(g):
         m_copy(g, 0).wait_recv()
         z_copy(g, 0).wait_recv()
         for way in (0, 1):
@@ -313,7 +328,6 @@
             def _():
                 m_copy(g, way).start()
                 z_copy(g, way).start()
-        dispatch(g)
 
     def plane_state():
         inc[...] = jnp.zeros_like(inc)
@@ -417,21 +431,53 @@
     near = [nth(n) for n in range(1, G)]
     for c in loads[8:]:
         c.wait()
-    arrive(near[0])
-    loads[2].wait()
-    for da in range(1, A):
-        o1_copy(da, tp).start()
-    for db in range(1, B):
-        o3_copy(0, db, tp).start()
-    plane_state()
-    arrive(near[1])
-    serve(near[0])
+    edge = (zi == 0) | (zi == G - 1)
     for da in range(1, A):
         o1_copy(da, shard(da)).wait_recv()
         for dy in range(1, R):
             o2_copy(da, dy, yi).start()
+    for db in range(1, B):
+        o3_copy(0, db, tp).start()
+    receive(near[0])
+
+    @pl.when(jnp.logical_not(edge))
+    def _():
+        receive(near[1])
+
+    dispatch(near[0])
+    plane_state()
+
+    @pl.when(edge)
+    def _():
+        receive(near[1])
+
+    dispatch(near[1])
+    @pl.when(jnp.logical_not(edge))
+    def _():
+        for g in near[2:]:
+            receive(g)
+    serve(near[0])
+    @pl.when(edge)
+    def _():
+        for g in near[2:]:
+            receive(g)
+
     for g in near[2:]:
-        arrive(g)
+        dispatch(g)
+    for da in range(1, A):
+        for dy in range(1, R):
+            o2_copy(da, dy, (yi + R - dy) % R).wait_recv()
+    oz_sends(zi)
+    serve(near[1])
+    oz_receive(near[0])
+    combine(near[0])
+    oz_receive(near[1])
+    @pl.when(jnp.logical_not(edge))
+    def _():
+        for g in near[2:]:
+            oz_receive(g)
+    for g in near[2:]:
+        serve(g)
     carried_state()
     loads[6].wait()
     loads[7].wait()
@@ -439,53 +485,75 @@
     @pl.loop(0, T)
     def _(i):
         retain(i, i // B, i % B)
-    serve(near[1])
-    for da in range(1, A):
-        for dy in range(1, R):
-            o2_copy(da, dy, (yi + R - dy) % R).wait_recv()
-        for dz in range(1, Q):
-            oz_copy(da, dz, zq).start()
-    combine(near[0])
-    for g in near[2:]:
-        serve(g)
+    for w in range(halves):
+        for da in range(1, A):
+            for db in range(B):
+                r_copy(da, db, w).start()
+        for db in range(1, B):
+            r_copy(0, db, w).start()
     serve(zi)
-    for da in range(1, A):
-        for db in range(B):
-            r_copy(da, db).start()
-    for db in range(1, B):
-        r_copy(0, db).start()
     combine(near[1])
     for g in near[2:]:
         combine(g)
+    @pl.when(edge)
+    def _():
+        for g in near[2:]:
+            oz_receive(g)
     for da in range(1, A):
-        for dz in range(1, Q):
-            oz_copy(da, dz, (zq + Q - dz) % Q).wait_recv()
         for db in range(1, B):
             o3_copy(da, db, shard(da)).start()
 
-    b_all(zi).wait_recv()
-    shr[...] += dot(dwt[zi], ret[zi])
-
     for db in range(1, B):
         o3_copy(0, db, shard(0, db)).wait_recv()
-        r_copy(0, db).wait_recv()
-
-    n_col = upd.shape[1]
+        for w in range(halves):
+            r_copy(0, db, w).wait_recv()
+
+    n_half = upd.shape[1]
+    n_col = 2 * n_half
     n_out = width // n_col
 
     def columns(n):
         return pl.ds(pl.multiple_of(n * n_col, n_col), n_col)
 
-    def out_rows(n):
-        return pl.ds(pl.multiple_of(n * mix_v.shape[0], mix_v.shape[0]), mix_v.shape[0])
+    def out_rows(n, part):
+        return pl.ds(pl.multiple_of((n * 2 + part) * strip, strip), strip)
 
     @pl.loop(0, n_out)
     def _(n):
         acc = dot(rs[0], op_v[tp, :, columns(n)])
         for db in range(1, B):
             acc += dot(rr[db - 1], op_v[shard(0, db), :, columns(n)])
-        upd[out_rows(n)] = acc
-
+        for w in range(2):
+            upd[out_rows(n, w)] = acc[:, w * n_half:(w + 1) * n_half]
+
+    def mix_out(n, part):
+        at = (strip_of(part), columns(n))
+        return pltpu.make_async_copy(mix_v.at[at], mix_hbm.at[at], mix_sem.at[n, part])
+
+    for w in range(halves):
+        for da in range(1, A):
+            for db in range(B):
+                if db and not w:
+                    o3_copy(da, db, shard(da, db)).wait_recv()
+                r_copy(da, db, w).wait_recv()
+
+                @pl.loop(0, n_out)
+                def _(n):
+                    acc = dot(rr[da * B + db - 1], op_v[shard(da, db), :, columns(n)])
+                    for w in range(2):
+                        at = slice(w * n_half, (w + 1) * n_half)
+                        part_sum = upd[out_rows(n, w)] + acc[:, at]
+                        if da == A - 1 and db == B - 1:
+                            mix_v[:, pl.ds(pl.multiple_of(n * n_col + w * n_half, n_half), n_half)] = (
+                                part_sum.astype(BF16)
+                            )
+                        else:
+                            upd[out_rows(n, w)] = part_sum
+                    if da == A - 1 and db == B - 1:
+                        mix_out(n, 0).start()
+
+    b_all(zi).wait_recv()
+    shr[...] += dot(dwt[zi], ret[zi])
     @pl.loop(1, G)
     def _(i):
         g = (zi + i) % G
@@ -495,28 +563,6 @@
     moe_v[...] = shr[...].astype(BF16)
     moe_out = pltpu.make_async_copy(moe_v, moe_hbm, moe_sem)
     moe_out.start()
-
-    def mix_out(n):
-        return pltpu.make_async_copy(
-            mix_v.at[:, columns(n)], mix_hbm.at[:, columns(n)], mix_sem.at[n]
-        )
-
-    for da in range(1, A):
-        for db in range(B):
-            if db:
-                o3_copy(da, db, shard(da, db)).wait_recv()
-            r_copy(da, db).wait_recv()
-
-            @pl.loop(0, n_out)
-            def _(n):
-                acc = upd[out_rows(n)] + dot(
-                    rr[da * B + db - 1], op_v[shard(da, db), :, columns(n)]
-                )
-                if da == A - 1 and db == B - 1:
-                    mix_v[:, columns(n)] = acc.astype(BF16)
-                    mix_out(n).start()
-                else:
-                    upd[out_rows(n)] = acc
 
     @pl.loop(0, G)
     def _(g):
@@ -551,15 +597,19 @@
     for da in range(A):
         for db in range(B):
             if da or db:
-                r_copy(da, db).wait_send()
+                for w in range(halves):
+                    r_copy(da, db, w).wait_send()
 
     for da in range(A):
         if da:
             o1_copy(da, tp).wait_send()
             for dy in range(1, R):
                 o2_copy(da, dy, yi).wait_send()
-            for dz in range(1, Q):
-                oz_copy(da, dz, zq).wait_send()
+            for g in range(G):
+                for way in (0, 1):
+                    @pl.when(z_sends(g, way))
+                    def _():
+                        oz_copy(da, g, way).wait_send()
         for db in range(1, B):
             o3_copy(da, db, shard(da)).wait_send()
 
@@ -567,7 +617,30 @@
 
     @pl.loop(0, n_out)
     def _(n):
-        mix_out(n).wait()
+        for w in range(halves):
+            mix_out(n, w).wait()
+
+
+def finish(mix_in, moe_in, mix_out, moe_out, mix_v, moe_v, in_sem, out_sem):
+    parts = in_sem.shape[0] - 1
+    strip = mix_v.shape[0] // parts
+
+    def pair(i):
+        if i == parts:
+            refs = (moe_in, moe_v, moe_out)
+        else:
+            refs = [r.at[i * strip:(i + 1) * strip] for r in (mix_in, mix_v, mix_out)]
+        return (pltpu.make_async_copy(refs[0], refs[1], in_sem.at[i]),
+                pltpu.make_async_copy(refs[1], refs[2], out_sem.at[i]))
+
+    pairs = [pair(i) for i in range(parts + 1)]
+    for load, _ in pairs:
+        load.start()
+    for load, store in pairs:
+        load.wait()
+        store.start()
+    for _, store in pairs:
+        store.wait()
 
 
 def local(
@@ -581,7 +654,6 @@
     Pn = R * T
     B = math.gcd(T, 2)
     A = T // B
-    Q = math.gcd(G, 2)
     n = query_rows.shape[0]
     H = query_rows.shape[1] // DK
     nb = n // BLOCK
@@ -611,15 +683,15 @@
         V((R, H, DK, DV), BF16), V((R, rows_t, 128), F32),
         V((G, H, DK, DV), BF16), V((G, rows_t, 128), F32), V((H, DK, DV), F32),
         V((T, rows_o, dvl), BF16), V((T - 1, rows_o, dvl), BF16), V((H, DK, DV), F32),
-        dma((12,)), dma((width // DV,)), dma,
+        dma((12,)), dma((width // DV, 2)), dma,
         dma((2, G)), dma((G,)), dma((2, G)), dma((G,)),
         dma((G,)), dma((G,)), dma((G,)), dma((G,)),
         dma((G,)), dma((G,)),
         dma((R,)), dma((R,)), dma((R,)), dma((R,)), dma((G,)), dma((G,)), dma((G,)), dma((G,)),
         dma((A,)), dma((A,)), dma((A, R)), dma((A, R)), dma((A, B)), dma((A, B)),
-        dma((A, Q)), dma((A, Q)), dma((T,)), dma((T,)),
+        dma((A, 2, G)), dma((A, G)), dma((T, 1)), dma((T, 1)),
     ]
-    return pl.pallas_call(
+    made = pl.pallas_call(
         functools.partial(kernel, E, T, G, C),
         out_shape=(
             jax.ShapeDtypeStruct((rows_o, width), BF16),
@@ -638,6 +710,17 @@
         expert_gate, expert_up, expert_down, shared_gate, shared_up, shared_down,
     )
 
+    parts = 8
+    return pl.pallas_call(
+        finish,
+        out_shape=tuple(jax.ShapeDtypeStruct(a.shape, a.dtype) for a in made),
+        in_specs=[hb] * 2,
+        out_specs=(hb, hb),
+        scratch_shapes=[V(a.shape, a.dtype) for a in made]
+        + [dma((parts + 1,)), dma((parts + 1,))],
+        name="finish",
+    )(*made)
+
 
 def solution(mesh):
     both = P(("ep", "tp"), None)

time: 149 us -> 137 us (0.919)
  Pallas kernels: 143 us -> 136 us
  local copies, waits for them, and re-layouts: 4.01 us -> 0 us
    pallas_call x1, Pallas kernels: 143 us -> 133 us  [local(): pl.pallas_call(functools.partial(kernel, E, T, G, C), out_shape=(jax.Shap...]
    unnamed x4 -> x0, local copies, waits for them, and re-layouts: 4.01 us -> none
    pallas_call x0 -> x1, Pallas kernels: none -> 2.63 us  [local(): pl.pallas_call(finish, out_shape=tuple((jax.ShapeDtypeStruct(a.shape, a.d...]
where the time goes in v3:
time: 137 us; the launch traced here: 136 us
  Pallas kernels  136 us (99%)
    pallas_call x1, Pallas kernels, local(): pl.pallas_call(functools.partial(kernel, E, T, G, C), out_shape=(jax.Shap...  133 us

profile of v3, /device:TPU:2, one launch (start us, length us, event | category | flops | bytes accessed | tf_op | source)
XLA Modules:
  0.0 136.5 jit_solution(16120853936984616263)
XLA Ops:
  0.6 133.2 %fused.1 = (bf16[512,2048]{1,0:T(8,128)(2,1)}, bf16[128,2048]{1,0:T(8,128)(2,1)}) custom-call(f32[1,2048]{1,0:T(1,128)} %bitcast.3, s32[4,128]{1,0:T(4,128)} %bitcast.4, f32[4,128]{1,0:T(4,128)} %bitcast.5, f32[2,2048]{1,0:T(2,128)} %decay_ref.1, bf16[128,2048]{1,0:T(8,128)(2,1)} %x_hbm.1, bf16[2048,256]{1,0:T(8,128)(2,1)} %q_hbm.1, ...), custom_call_target="tpu_custom_call" | custom-call | tf_op jit(solution)/shard_map/fused/pallas_call | solution.py:694
  133.9 2.6 %finish.1 = (bf16[512,2048]{1,0:T(8,128)(2,1)}, bf16[128,2048]{1,0:T(8,128)(2,1)}) custom-call(bf16[512,2048]{1,0:T(8,128)(2,1)} %get-tuple-element.4.mix_in, bf16[128,2048]{1,0:T(8,128)(2,1)} %get-tuple-element.5.moe_in), custom_call_target="tpu_custom_call" | custom-call | tf_op jit(solution)/shard_map/finish/pallas_call | solution.py:714

commit v4 on v3

--- a/solution.py
+++ b/solution.py
@@ -36,9 +36,9 @@
     x_v, mix_v, moe_v, cum_ref, cumc_ref,
     q_v, k_v, v_v, g_v, op_v, wg_v, wu_v, wd_v,
     xz, mz, dsp, rcv, ret, dwt, shr, prcv,
-    upd, sblk, srcv, trcv, zrcv, ztot, pre, rs, rr, inc,
+    upd, sblk, srcv, trcv, zrcv, pre, rs, rr, inc,
     load_sem, mix_sem, moe_sem,
-    z_s, z_r, m_s, m_r, d_s, d_r, b_s, b_r, p_s, p_r, s_s, s_r, t_s, t_r, e_s, e_r, f_s, f_r,
+    z_s, z_r, m_s, m_r, d_s, d_r, b_s, b_r, p_s, p_r, s_s, s_r, t_s, t_r, e_s, e_r,
     o1_s, o1_r, o2_s, o2_r, o3_s, o3_r, oz_s, oz_r, r_s, r_r,
 ):
     ep = lax.axis_index("ep")
@@ -154,11 +154,8 @@
         return rcopy(trcv.at[0], trcv.at[d], t_s.at[d], t_r.at[d],
                      (zi * R + (yi + d) % R, tp))
 
-    def e_copy(d):
-        return rcopy(zrcv.at[0], zrcv.at[d], e_s.at[d], e_r.at[d], z_place((zi + d) % G))
-
-    def f_copy(d):
-        return rcopy(ztot.at[0], ztot.at[d], f_s.at[d], f_r.at[d], z_place((zi + d) % G))
+    def e_copy():
+        return rcopy(zrcv.at[0], zrcv.at[1], e_s, e_r, z_place(zi + 1))
 
     def shard(da, db=0):
         return ((ta + A - da) % A) * B + (tb + B - db) % B
@@ -308,17 +305,28 @@
     for c in loads[8:]:
         c.start()
 
-    def serve(r):
+    def give_back(r, wanted):
+        @pl.loop(1, Pn)
+        def _(d):
+            @pl.when(wanted(d))
+            def _():
+                b_copy(r, d).start()
+
+    def early(d):
+        return d % T != T // 2
+
+    def late(d):
+        return d % T == T // 2
+
+    def serve(r, *wanted):
         d_all(r).wait_recv()
         rows_in = rcv[r]
         hidden = (silu(dot(rows_in, wg_v[...])) * dot(rows_in, wu_v[...])).astype(BF16)
         res = dot(hidden, wd_v[...]).astype(BF16)
         rcv[r] = res
         ret[r, 0:C] = res[0:C]
-
-        @pl.loop(1, Pn)
-        def _(d):
-            b_copy(r, d).start()
+        for want in wanted or (early, late):
+            give_back(r, want)
 
     def receive(g):
         m_copy(g, 0).wait_recv()
@@ -331,13 +339,11 @@
 
     def plane_state():
         inc[...] = jnp.zeros_like(inc)
-        ztot[0] = trcv[0]
 
         @pl.loop(1, R)
         def _(d):
             t_copy(d).wait_recv()
             s_copy(d).wait_recv()
-            ztot[0] += trcv[d]
 
         @pl.loop(0, R)
         def _(y):
@@ -352,26 +358,37 @@
 
         zrcv[0] = inc[...].astype(BF16)
 
-        @pl.loop(1, G)
-        def _(d):
-            @pl.when(zi + d < G)
+        @pl.when((zi == 0) & (zi + 1 < G))
+        def _():
+            e_copy().start()
+
+    def carry(k):
+        @pl.when(zi == k)
+        def _():
+            e_copy().wait_recv()
+            inc[...] = zrcv[1].astype(F32)
+
+            @pl.loop(0, R)
+            def _(y):
+                for h in range(H):
+                    inc[h] = inc[h] * jnp.exp(trcv[y, h:h + 1, 0:1])
+
+            inc[...] += zrcv[0].astype(F32)
+            zrcv[0] = inc[...].astype(BF16)
+            e_copy().start()
+
+    def carried_state():
+        @pl.when(zi == 0)
+        def _():
+            inc[...] = jnp.zeros_like(inc)
+
+        @pl.when(zi > 0)
+        def _():
+            @pl.when(zi == G - 1)
             def _():
-                f_copy(d).start()
-                e_copy(d).start()
-
-    def carried_state():
-        inc[...] = jnp.zeros_like(inc)
-
-        @pl.loop(1, G)
-        def _(i):
-            d = G - i
-
-            @pl.when(zi >= d)
-            def _():
-                f_copy(d).wait_recv()
-                e_copy(d).wait_recv()
-                for h in range(H):
-                    inc[h] = inc[h] * jnp.exp(ztot[d, h:h + 1, 0:1]) + zrcv[d, h].astype(F32)
+                e_copy().wait_recv()
+
+            inc[...] = zrcv[1].astype(F32)
 
         @pl.loop(0, R)
         def _(y):
@@ -456,7 +473,12 @@
     def _():
         for g in near[2:]:
             receive(g)
+    for da in range(1, A):
+        for dy in range(1, R):
+            o2_copy(da, dy, (yi + R - dy) % R).wait_recv()
+    oz_sends(zi)
     serve(near[0])
+    carry(1)
     @pl.when(edge)
     def _():
         for g in near[2:]:
@@ -464,34 +486,32 @@
 
     for g in near[2:]:
         dispatch(g)
-    for da in range(1, A):
-        for dy in range(1, R):
-            o2_copy(da, dy, (yi + R - dy) % R).wait_recv()
-    oz_sends(zi)
     serve(near[1])
+    carry(2)
     oz_receive(near[0])
     combine(near[0])
+    serve(zi, early)
     oz_receive(near[1])
+    carried_state()
+    loads[6].wait()
+    loads[7].wait()
+
+    @pl.loop(0, T)
+    def _(i):
+        retain(i, i // B, i % B)
+    for g in near[2:]:
+        serve(g)
     @pl.when(jnp.logical_not(edge))
     def _():
         for g in near[2:]:
             oz_receive(g)
-    for g in near[2:]:
-        serve(g)
-    carried_state()
-    loads[6].wait()
-    loads[7].wait()
-
-    @pl.loop(0, T)
-    def _(i):
-        retain(i, i // B, i % B)
     for w in range(halves):
         for da in range(1, A):
             for db in range(B):
                 r_copy(da, db, w).start()
         for db in range(1, B):
             r_copy(0, db, w).start()
-    serve(zi)
+    give_back(zi, late)
     combine(near[1])
     for g in near[2:]:
         combine(g)
@@ -587,12 +607,9 @@
         t_copy(d).wait_send()
         s_copy(d).wait_send()
 
-    @pl.loop(1, G)
-    def _(d):
-        @pl.when(zi + d < G)
-        def _():
-            f_copy(d).wait_send()
-            e_copy(d).wait_send()
+    @pl.when(zi + 1 < G)
+    def _():
+        e_copy().wait_send()
 
     for da in range(A):
         for db in range(B):
@@ -662,6 +679,7 @@
     C = 2 * tok * visits // (E * T)
     ff = expert_gate.shape[2]
     assert shared_gate.shape[1] == ff
+    assert G == Z_GROUPS
     rows_o = n // T
     dvl = H * DV
 
@@ -681,13 +699,13 @@
         V((G, tok, Pn * C), BF16), V((tok, width), F32), V((G, tok, width), BF16),
         V((max(nb * H * DK, rows_o * width // DV), DV), F32), V((nb, H, DK, DV), BF16),
         V((R, H, DK, DV), BF16), V((R, rows_t, 128), F32),
-        V((G, H, DK, DV), BF16), V((G, rows_t, 128), F32), V((H, DK, DV), F32),
+        V((2, H, DK, DV), BF16), V((H, DK, DV), F32),
         V((T, rows_o, dvl), BF16), V((T - 1, rows_o, dvl), BF16), V((H, DK, DV), F32),
         dma((12,)), dma((width // DV, 2)), dma,
         dma((2, G)), dma((G,)), dma((2, G)), dma((G,)),
         dma((G,)), dma((G,)), dma((G,)), dma((G,)),
         dma((G,)), dma((G,)),
-        dma((R,)), dma((R,)), dma((R,)), dma((R,)), dma((G,)), dma((G,)), dma((G,)), dma((G,)),
+        dma((R,)), dma((R,)), dma((R,)), dma((R,)), dma, dma,
         dma((A,)), dma((A,)), dma((A, R)), dma((A, R)), dma((A, B)), dma((A, B)),
         dma((A, 2, G)), dma((A, G)), dma((T, 1)), dma((T, 1)),
     ]

time: 137 us -> 136 us (level)
  no operation moved by 1% of the time
where the time goes in v4:
time: 136 us; the launch traced here: 135 us
  Pallas kernels  135 us (99%)
    pallas_call x1, Pallas kernels, local(): pl.pallas_call(functools.partial(kernel, E, T, G, C), out_shape=(jax.Shap...  132 us

profile of v4, /device:TPU:2, one launch (start us, length us, event | category | flops | bytes accessed | tf_op | source)
XLA Modules:
  0.0 135.3 jit_solution(12658730097705334226)
XLA Ops:
  0.6 131.9 %fused.1 = (bf16[512,2048]{1,0:T(8,128)(2,1)}, bf16[128,2048]{1,0:T(8,128)(2,1)}) custom-call(f32[1,2048]{1,0:T(1,128)} %bitcast.3, s32[4,128]{1,0:T(4,128)} %bitcast.4, f32[4,128]{1,0:T(4,128)} %bitcast.5, f32[2,2048]{1,0:T(2,128)} %decay_ref.1, bf16[128,2048]{1,0:T(8,128)(2,1)} %x_hbm.1, bf16[2048,256]{1,0:T(8,128)(2,1)} %q_hbm.1, ...), custom_call_target="tpu_custom_call" | custom-call | tf_op jit(solution)/shard_map/fused/pallas_call | solution.py:712
  132.5 2.6 %finish.1 = (bf16[512,2048]{1,0:T(8,128)(2,1)}, bf16[128,2048]{1,0:T(8,128)(2,1)}) custom-call(bf16[512,2048]{1,0:T(8,128)(2,1)} %get-tuple-element.4.mix_in, bf16[128,2048]{1,0:T(8,128)(2,1)} %get-tuple-element.5.moe_in), custom_call_target="tpu_custom_call" | custom-call | tf_op jit(solution)/shard_map/finish/pallas_call | solution.py:732

commit v5 on v4

--- a/solution.py
+++ b/solution.py
@@ -490,7 +490,6 @@
     carry(2)
     oz_receive(near[0])
     combine(near[0])
-    serve(zi, early)
     oz_receive(near[1])
     carried_state()
     loads[6].wait()
@@ -499,12 +498,14 @@
     @pl.loop(0, T)
     def _(i):
         retain(i, i // B, i % B)
+    serve(zi, early)
     for g in near[2:]:
         serve(g)
     @pl.when(jnp.logical_not(edge))
     def _():
         for g in near[2:]:
             oz_receive(g)
+    combine(near[1])
     for w in range(halves):
         for da in range(1, A):
             for db in range(B):
@@ -512,7 +513,6 @@
         for db in range(1, B):
             r_copy(0, db, w).start()
     give_back(zi, late)
-    combine(near[1])
     for g in near[2:]:
         combine(g)
     @pl.when(edge)

time: 136 us -> 134 us (0.985)
  Pallas kernels: 135 us -> 133 us
    pallas_call x1, Pallas kernels: 132 us -> 130 us  [local(): pl.pallas_call(functools.partial(kernel, E, T, G, C), out_shape=(jax.Shap...]
where the time goes in v5:
time: 134 us
  Pallas kernels  133 us (99%)
    pallas_call x1, Pallas kernels, local(): pl.pallas_call(functools.partial(kernel, E, T, G, C), out_shape=(jax.Shap...  130 us

profile of v5, /device:TPU:2, one launch (start us, length us, event | category | flops | bytes accessed | tf_op | source)
XLA Modules:
  0.0 133.9 jit_solution(16538707565020285483)
XLA Ops:
  0.6 130.5 %fused.1 = (bf16[512,2048]{1,0:T(8,128)(2,1)}, bf16[128,2048]{1,0:T(8,128)(2,1)}) custom-call(f32[1,2048]{1,0:T(1,128)} %bitcast.3, s32[4,128]{1,0:T(4,128)} %bitcast.4, f32[4,128]{1,0:T(4,128)} %bitcast.5, f32[2,2048]{1,0:T(2,128)} %decay_ref.1, bf16[128,2048]{1,0:T(8,128)(2,1)} %x_hbm.1, bf16[2048,256]{1,0:T(8,128)(2,1)} %q_hbm.1, ...), custom_call_target="tpu_custom_call" | custom-call | tf_op jit(solution)/shard_map/fused/pallas_call | solution.py:712
  131.1 2.6 %finish.1 = (bf16[512,2048]{1,0:T(8,128)(2,1)}, bf16[128,2048]{1,0:T(8,128)(2,1)}) custom-call(bf16[512,2048]{1,0:T(8,128)(2,1)} %get-tuple-element.4.mix_in, bf16[128,2048]{1,0:T(8,128)(2,1)} %get-tuple-element.5.moe_in), custom_call_target="tpu_custom_call" | custom-call | tf_op jit(solution)/shard_map/finish/pallas_call | solution.py:732
